TPU v7x, 32 devices: a whole 2x2x4 slice. The times are simulated.
32 devices in a mesh: ep: 8 (over z, y), tp: 4 (over x, core).
Axes of the slice: x: 2, y: 2, z: 4, core: 2. Of those that a mesh axis runs over, the one named last changes fastest.
Arguments:
- tokens: bfloat16 [2048, 2048], P('ep'), may hold values from -6 to 6
- cotangent: bfloat16 [2048, 2048], P('ep'), may hold values from -6 to 6
- gate_weights: bfloat16 [2048, 2], P('ep'), may hold values from 0.099609375 to 0.8984375
- routes: int32 [2048, 2], P('ep'), may hold values from 0 to 7, all different within a row; in each aligned block of 256 rows (0 to 255, 256 to 511, ...) at most 96 rows name the same one
- w_gate: bfloat16 [8, 2048, 3584], P('ep', None, 'tp'), may hold values from -0.125 to 0.125
- w_up: bfloat16 [8, 2048, 3584], P('ep', None, 'tp'), may hold values from -0.125 to 0.125
- w_down: bfloat16 [8, 3584, 2048], P('ep', 'tp'), may hold values from -0.09375 to 0.09375
Outputs:
- grad_tokens: bfloat16 [2048, 2048], P('ep', 'tp')
- grad_gates: float32 [2048, 2], P('ep')
- grad_w_gate: bfloat16 [8, 2048, 3584], P('ep', None, 'tp')
- grad_w_up: bfloat16 [8, 2048, 3584], P('ep', None, 'tp')
- grad_w_down: bfloat16 [8, 3584, 2048], P('ep', 'tp')
Inputs may be any that keep to these rules, and one draw needn't show every extreme that they name: `routes`: each row names 2 different experts. Among the rows of one index of ep no expert is named by more than 96 rows, and this bound is reached in every draw.
All inputs are finite; a program needn't handle non-finite values.
Results may differ from a plain program's by a relative error of at most 0.012.
Values may be sent and summed in bfloat16 or wider, within the bound.
A program may use at most 128 MiB of HBM per device.

v0:
```python
import functools

import jax
import jax.numpy as jnp
from jax import lax
from jax.experimental import pallas as pl
from jax.experimental.pallas import tpu as pltpu
from jax.sharding import PartitionSpec as P

MESH = pl.DeviceIdType.MESH
LAST = (((1,), (1,)), ((), ()))
FIRST = (((0,), (0,)), ((), ()))
GATE_ROWS = 16
SUM_ROWS = 8


def expert_kernel(groups, slot, quarter,
                  sent_tok, sent_cot, sent_gate, w_gate, w_up, w_down,
                  back_rows, back_gate, out_gate, out_up, out_down,
                  x_rows, c_rows, gates, wg, wu, wd, gate_pre, up_pre, back, hidden, grads,
                  part, core_got, x_got, total, gate_all, gate_sum,
                  og, ou, od,
                  load_sem, near_sem, first_send, first_recv, core_send, core_recv,
                  x_send, x_recv, second_send, second_recv, gate_send, gate_recv,
                  pair_send, pair_recv, cross_send, cross_recv, home_send, home_recv,
                  sum_send, sum_recv, sumhome_send, sumhome_recv, out_sem):
    me = lax.axis_index("ep")
    t = lax.axis_index("tp")
    core = lax.rem(t, 2)
    side = t // 2
    core_peer = side * 2 + (1 - core)
    x_peer = (1 - side) * 2 + core
    rows = groups * slot
    ffe = wg.shape[1]
    width = wg.shape[0]

    barrier = pltpu.get_barrier_semaphore()

    def greet(d, _):
        pl.semaphore_signal(barrier, inc=1, device_id=(lax.rem(me + d, groups), t),
                            device_id_type=MESH)
        return 0

    loads = [
        pltpu.make_async_copy(w_gate, wg, load_sem.at[0]),
        pltpu.make_async_copy(w_up, wu, load_sem.at[1]),
        pltpu.make_async_copy(w_down, wd, load_sem.at[2]),
    ]
    lax.fori_loop(1, groups, greet, 0)
    for o in range(1, 4):
        pl.semaphore_signal(barrier, inc=1, device_id=(me, lax.rem(t + o, 4)),
                            device_id_type=MESH)
    for load in loads:
        load.start()
    pl.semaphore_wait(barrier, groups + 2)

    def rblk(ref, s, size=slot):
        return ref.at[pl.ds(pl.multiple_of(s * size, size if size < 16 else 16), size)]

    def blk(ref, s, q):
        return ref.at[pl.ds(pl.multiple_of(s * slot, 16), slot),
                      pl.ds(pl.multiple_of(q * quarter, 128), quarter)]

    def rc(src, dst, ssem, rsem, ep, tp):
        return pltpu.make_async_remote_copy(
            src_ref=src, dst_ref=dst, send_sem=ssem, recv_sem=rsem,
            device_id=(ep, tp), device_id_type=MESH)

    def loop(lo, hi, body):
        def step(d, c):
            body(d)
            return c
        lax.fori_loop(lo, hi, step, 0)

    sent = (sent_tok, sent_cot)
    full = (x_rows, c_rows)

    def first(a, d, land):
        to = lax.rem(me + d, groups)
        return rc(rblk(sent[a], to), blk(full[a], land, t), first_send.at[a, d],
                  first_recv.at[a, d], to, t)

    def gate_copy(d, land):
        to = lax.rem(me + d, groups)
        return rc(rblk(sent_gate, to, GATE_ROWS), rblk(gates, land, GATE_ROWS),
                  gate_send.at[d], gate_recv.at[d], to, t)

    def source(d):
        return lax.rem(me - d + groups, groups)

    def to_core(a, d, q):
        s = source(d)
        return rc(blk(full[a], s, q), blk(full[a], s, q), core_send.at[a, d],
                  core_recv.at[a, d], me, core_peer)

    def to_x(a, d, q):
        s = source(d)
        return rc(blk(full[a], s, q), blk(full[a], s, q), x_send.at[a, d],
                  x_recv.at[a, d], me, x_peer)

    def to_core_again(a, d, q):
        s = source(d)
        return rc(blk(full[a], s, q), blk(full[a], s, q), second_send.at[a, d],
                  second_recv.at[a, d], me, core_peer)

    x_core_peer = (1 - side) * 2 + (1 - core)

    for a in range(2):
        loop(1, groups, lambda d, a=a: first(a, d, me).start())
        if a == 0:
            loop(1, groups, lambda d: gate_copy(d, me).start())
    near = [pltpu.make_async_copy(rblk(sent[a], me), blk(full[a], me, t), near_sem.at[a])
            for a in range(2)]
    near.append(pltpu.make_async_copy(rblk(sent_gate, me, GATE_ROWS), rblk(gates, me, GATE_ROWS),
                                      near_sem.at[2]))
    for copy in near:
        copy.start()
    for copy in near:
        copy.wait()

    def forward(a, d):
        to_x(a, d, t).start()
        to_core(a, d, t).start()

    def stage1(a, d):
        first(a, d, source(d)).wait_recv()
        forward(a, d)

    def stage2(a, d):
        to_x(a, d, x_peer).wait_recv()
        to_core_again(a, d, x_peer).start()

    def settle(a):
        def body(d):
            to_core(a, d, core_peer).wait_recv()
            to_core_again(a, d, x_core_peer).wait_recv()
        loop(0, groups, body)

    def both(a):
        def body(d):
            stage1(a, d)
            stage2(a, d - 1)
        return body

    forward(0, 0)
    loop(1, groups, both(0))
    stage2(0, groups - 1)
    forward(1, 0)
    settle(0)
    loads[0].wait()
    loads[1].wait()

    half = rows // 2
    chunks = []
    at = 0
    while at < ffe:
        chunks.append((at, min(256, ffe - at)))
        at += 256
    pieces = [(w, o, lo, n) for lo, n in chunks for w, o in ((wg, gate_pre), (wu, up_pre))]

    def product(lhs, w, o, lo, n):
        def body(h):
            r = pl.ds(pl.multiple_of(h * half, 16), half)
            o[r, lo:lo + n] = jnp.dot(lhs[r, :], w[:, lo:lo + n],
                                      preferred_element_type=jnp.float32)
        loop(0, 2, body)

    count = len(pieces)
    for i, (w, o, lo, n) in enumerate(pieces):
        product(x_rows, w, o, lo, n)
        lower, upper = max(1, i * groups // count), (i + 1) * groups // count
        if upper > lower:
            loop(lower, upper, both(1))
    stage2(1, groups - 1)
    settle(1)
    loop(1, groups, lambda d: gate_copy(d, source(d)).wait_recv())
    loads[2].wait()

    def back_product(lo, n):
        def body(h):
            r = pl.ds(pl.multiple_of(h * half, 16), half)
            back[r, lo:lo + n] = lax.dot_general(
                c_rows[r, :], wd[lo:lo + n, :], LAST, preferred_element_type=jnp.float32)
        loop(0, 2, body)

    for lo, n in chunks:
        back_product(lo, n)

    lanes = gates.shape[1]
    eye = (lax.broadcasted_iota(jnp.int32, (slot, lanes), 0)
           == lax.broadcasted_iota(jnp.int32, (slot, lanes), 1)).astype(jnp.bfloat16)

    def weight_of(s):
        g = gates[pl.ds(pl.multiple_of(s * GATE_ROWS, GATE_ROWS), GATE_ROWS), :]
        return lax.dot_general(eye, g, LAST, preferred_element_type=jnp.float32)[:, 0:1]

    def elementwise(s):
        r = pl.ds(pl.multiple_of(s * slot, 16), slot)
        weight = weight_of(s)
        summed = jnp.zeros((slot, 128), jnp.float32)
        for lo in range(0, ffe, 128):
            g = gate_pre[r, lo:lo + 128]
            u = up_pre[r, lo:lo + 128]
            b = back[r, lo:lo + 128]
            logistic = jax.nn.sigmoid(g)
            act = g * logistic
            h = (act * u).astype(jnp.bfloat16)
            hidden[r, lo:lo + 128] = h
            summed = summed + h.astype(jnp.float32) * b
            gh = weight * b
            grads[r, lo:lo + 128] = (gh * u * logistic * (1.0 + g * (1.0 - logistic))).astype(
                jnp.bfloat16)
            grads[r, ffe + lo:ffe + lo + 128] = (gh * act).astype(jnp.bfloat16)
        padded = jnp.concatenate(
            [summed, jnp.zeros((lanes - slot, 128), jnp.float32)], axis=0) if lanes > slot else summed
        row = jnp.sum(padded.T, axis=0, keepdims=True)
        gate_all[t, pl.ds(pl.multiple_of(s * SUM_ROWS, SUM_ROWS), SUM_ROWS), :] = jnp.broadcast_to(
            row, (SUM_ROWS, lanes))
        cs = c_rows[r, :].astype(jnp.float32) * weight
        c_rows[r, :] = cs.astype(jnp.bfloat16)

    def drain(a):
        def body(d):
            to_core(a, d, t).wait_send()
            to_x(a, d, t).wait_send()
            to_core_again(a, d, x_peer).wait_send()
        loop(0, groups, body)
        loop(1, groups, lambda d: first(a, d, me).wait_send())

    drain(1)
    loop(0, groups, elementwise)

    sums = [rc(gate_all.at[t], gate_all.at[t], sum_send.at[o - 1], sum_recv.at[o - 1],
               me, lax.rem(t + o, 4)) for o in range(1, 4)]
    for copy in sums:
        copy.start()

    def row_product(q, store):
        cols = pl.ds(pl.multiple_of(q * quarter, 128), quarter)

        def body(h):
            r = pl.ds(pl.multiple_of(h * half, 16), half)
            value = lax.dot_general(grads[r, 0:ffe], wg[cols, :], LAST,
                                    preferred_element_type=jnp.float32)
            value = value + lax.dot_general(grads[r, ffe:2 * ffe], wu[cols, :], LAST,
                                            preferred_element_type=jnp.float32)
            store(r, value.astype(jnp.bfloat16))
        loop(0, 2, body)

    def store_part(i):
        def store(r, value):
            part[i, r, :] = value
        return store

    pairs = [rc(part.at[i], core_got.at[i], pair_send.at[i], pair_recv.at[i], me, core_peer)
             for i in range(2)]
    row_product((1 - side) * 2 + (1 - core), store_part(0))
    pairs[0].start()
    row_product(x_peer, store_part(2))
    pairs[0].wait_recv()

    def cross(s):
        return rc(rblk(part.at[2], s), rblk(x_got, s), cross_send.at[s], cross_recv.at[s],
                  me, x_peer)

    def add_cross(d):
        s = lax.rem(me + d, groups)
        r = pl.ds(pl.multiple_of(s * slot, 16), slot)
        part[2, r, :] = (part[2, r, :].astype(jnp.float32)
                         + core_got[0, r, :].astype(jnp.float32)).astype(jnp.bfloat16)
        cross(s).start()

    loop(1, groups + 1, add_cross)
    row_product(side * 2 + (1 - core), store_part(1))
    pairs[1].start()
    row_product(t, store_part(3))
    for copy in sums:
        copy.wait_recv()
    gate_sum[...] = (gate_all[0] + gate_all[1]) + (gate_all[2] + gate_all[3])

    def sum_home(d, land):
        to = lax.rem(me + d, groups)
        return rc(rblk(gate_sum, to, SUM_ROWS), rblk(back_gate, land, SUM_ROWS),
                  sumhome_send.at[d], sumhome_recv.at[d], to, t)

    loop(1, groups, lambda d: sum_home(d, me).start())
    last = pltpu.make_async_copy(rblk(gate_sum, me, SUM_ROWS), rblk(back_gate, me, SUM_ROWS),
                                 near_sem.at[2])
    last.start()
    pairs[1].wait_recv()

    def home(d, land):
        to = lax.rem(me + d, groups)
        return rc(rblk(total, to), rblk(back_rows, land), home_send.at[d], home_recv.at[d], to, t)

    def finish(d):
        s = lax.rem(me + d, groups)
        r = pl.ds(pl.multiple_of(s * slot, 16), slot)
        cross(s).wait_recv()
        total[r, :] = (part[3, r, :].astype(jnp.float32) + core_got[1, r, :].astype(jnp.float32)
                       + x_got[r, :].astype(jnp.float32)).astype(jnp.bfloat16)

    def finish_send(d):
        finish(d)
        home(d, me).start()

    outs = []
    work = []

    def x_grad(lo, n, i):
        def run():
            left = x_rows[:, lo:lo + n]
            og[lo:lo + n, :] = lax.dot_general(
                left, grads[:, 0:ffe], FIRST, preferred_element_type=jnp.float32
            ).astype(jnp.bfloat16)
            ou[lo:lo + n, :] = lax.dot_general(
                left, grads[:, ffe:2 * ffe], FIRST, preferred_element_type=jnp.float32
            ).astype(jnp.bfloat16)
            for j, (src, dst) in enumerate(((og, out_gate), (ou, out_up))):
                copy = pltpu.make_async_copy(src.at[lo:lo + n], dst.at[lo:lo + n],
                                             out_sem.at[i, j])
                copy.start()
                outs.append(copy)
        return run

    def down_grad(lo, n, i):
        def run():
            od[lo:lo + n, :] = lax.dot_general(
                hidden[:, lo:lo + n], c_rows[...], FIRST, preferred_element_type=jnp.float32
            ).astype(jnp.bfloat16)
            copy = pltpu.make_async_copy(od.at[lo:lo + n], out_down.at[lo:lo + n],
                                         out_sem.at[i, 2])
            copy.start()
            outs.append(copy)
        return run

    step = 256
    for i, lo in enumerate(range(0, width, step)):
        work.append(x_grad(lo, min(step, width - lo), i))
    for i, (lo, n) in enumerate(chunks):
        work.append(down_grad(lo, n, i))
    lead = len(work) - 1
    for i, run in enumerate(work):
        run()
        lower, upper = max(1, 1 + i * (groups - 1) // lead), min(groups, 1 + (i + 1) * (groups - 1) // lead)
        if upper > lower:
            loop(lower, upper, finish_send)
    finish(0)
    own = pltpu.make_async_copy(rblk(total, me), rblk(back_rows, me), near_sem.at[0])
    own.start()

    loop(1, groups, lambda d: home(d, source(d)).wait_recv())
    loop(1, groups, lambda d: sum_home(d, source(d)).wait_recv())
    own.wait()
    last.wait()
    drain(0)
    loop(1, groups, lambda d: gate_copy(d, me).wait_send())
    for copy in sums + pairs:
        copy.wait_send()
    loop(0, groups, lambda s: cross(s).wait_send())
    loop(1, groups, lambda d: home(d, me).wait_send())
    loop(1, groups, lambda d: sum_home(d, me).wait_send())
    for copy in outs:
        copy.wait()


def on_device(tokens, cotangent, gate_weights, routes, w_gate, w_up, w_down):
    tok_dev, width = tokens.shape
    top_k = routes.shape[1]
    groups = lax.axis_size("ep")
    narrow = lax.axis_size("tp")
    pair_count = tok_dev * top_k
    capacity = 3 * top_k * tok_dev // (2 * groups)
    slot = -(-capacity // 16) * 16
    quarter = width // narrow
    ffe = w_gate.shape[2]
    rows = groups * slot
    lanes = -(-slot // 128) * 128
    routed = routes.reshape(pair_count)
    onehot = (routed[:, None] == jnp.arange(groups, dtype=jnp.int32)[None, :])
    before = (jnp.arange(pair_count, dtype=jnp.int32)[:, None]
              > jnp.arange(pair_count, dtype=jnp.int32)[None, :])
    counts = jnp.dot(before.astype(jnp.bfloat16), onehot.astype(jnp.bfloat16),
                     preferred_element_type=jnp.float32).astype(jnp.int32)
    earlier = jnp.sum(jnp.where(onehot, counts, 0), axis=1)
    slot_of = (routed * slot + earlier).reshape(tok_dev, top_k)
    places = jnp.arange(rows, dtype=jnp.int32)
    hits = [slot_of[:, k][:, None] == places[None, :] for k in range(top_k)]
    picked = hits[0]
    for hit in hits[1:]:
        picked = picked | hit
    select = picked.astype(jnp.bfloat16)
    offset = lax.axis_index("tp") * quarter
    tok_part = lax.dynamic_slice_in_dim(tokens, offset, quarter, 1)
    cot_part = lax.dynamic_slice_in_dim(cotangent, offset, quarter, 1)
    contract_first = (((0,), (0,)), ((), ()))
    sent_tok = lax.dot_general(select, tok_part, contract_first,
                               preferred_element_type=jnp.float32).astype(jnp.bfloat16)
    sent_cot = lax.dot_general(select, cot_part, contract_first,
                               preferred_element_type=jnp.float32).astype(jnp.bfloat16)
    gate_row = jnp.zeros((rows,), jnp.float32)
    for k in range(top_k):
        gate_row = gate_row + jnp.sum(
            jnp.where(hits[k], gate_weights[:, k].astype(jnp.float32)[:, None], 0.0), axis=0)
    sent_gate = jnp.pad(gate_row.reshape(groups, slot), ((0, 0), (0, lanes - slot)))
    sent_gate = jnp.broadcast_to(
        sent_gate.astype(jnp.bfloat16)[:, None, :], (groups, GATE_ROWS, lanes)
    ).reshape(groups * GATE_ROWS, lanes)
    vmem = pl.BlockSpec(memory_space=pltpu.VMEM)
    hbm = pl.BlockSpec(memory_space=pl.ANY)
    bf, f32 = jnp.bfloat16, jnp.float32
    dma = pltpu.SemaphoreType.DMA
    per = dma((groups,))
    twice = dma((2, groups))
    steps = max(-(-width // 256), -(-ffe // 256))
    back_rows, back_gate, grad_gate_w, grad_up_w, grad_down = pl.pallas_call(
        functools.partial(expert_kernel, groups, slot, quarter),
        out_shape=(
            jax.ShapeDtypeStruct((rows, quarter), bf),
            jax.ShapeDtypeStruct((groups * SUM_ROWS, lanes), f32),
            jax.ShapeDtypeStruct((width, ffe), bf),
            jax.ShapeDtypeStruct((width, ffe), bf),
            jax.ShapeDtypeStruct((ffe, width), bf),
        ),
        in_specs=[vmem, vmem, vmem, hbm, hbm, hbm],
        out_specs=(vmem, vmem, hbm, hbm, hbm),
        scratch_shapes=[
            pltpu.VMEM((rows, width), bf),
            pltpu.VMEM((rows, width), bf),
            pltpu.VMEM((groups * GATE_ROWS, lanes), bf),
            pltpu.VMEM((width, ffe), bf),
            pltpu.VMEM((width, ffe), bf),
            pltpu.VMEM((ffe, width), bf),
            pltpu.VMEM((rows, ffe), f32),
            pltpu.VMEM((rows, ffe), f32),
            pltpu.VMEM((rows, ffe), f32),
            pltpu.VMEM((rows, ffe), bf),
            pltpu.VMEM((rows, 2 * ffe), bf),
            pltpu.VMEM((4, rows, quarter), bf),
            pltpu.VMEM((2, rows, quarter), bf),
            pltpu.VMEM((rows, quarter), bf),
            pltpu.VMEM((rows, quarter), bf),
            pltpu.VMEM((4, groups * SUM_ROWS, lanes), f32),
            pltpu.VMEM((groups * SUM_ROWS, lanes), f32),
            pltpu.VMEM((width, ffe), bf),
            pltpu.VMEM((width, ffe), bf),
            pltpu.VMEM((ffe, width), bf),
            dma((3,)), dma((3,)),
            twice, twice, twice, twice, twice, twice, twice, twice,
            per, per,
            dma((2,)), dma((2,)),
            per, per, per, per,
            dma((3,)), dma((3,)),
            per, per,
            dma((steps, 3)),
        ],
        compiler_params=pltpu.CompilerParams(
            collective_id=0, has_side_effects=True, vmem_limit_bytes=67043328),
    )(sent_tok, sent_cot, sent_gate, w_gate[0], w_up[0], w_down[0])
    grad_tokens = jnp.dot(select, back_rows, preferred_element_type=f32).astype(bf)
    gate_line = back_gate.reshape(groups, SUM_ROWS, lanes)[:, 0, :slot].reshape(rows)
    grad_gates = jnp.stack(
        [jnp.sum(jnp.where(hit, gate_line[None, :], 0.0), axis=1) for hit in hits], axis=1)
    return (grad_tokens, grad_gates, grad_gate_w[None], grad_up_w[None], grad_down[None])


def solution(mesh):
    in_specs = (
        P("ep", None),
        P("ep", None),
        P("ep", None),
        P("ep", None),
        P("ep", None, "tp"),
        P("ep", None, "tp"),
        P("ep", "tp", None),
    )
    out_specs = (
        P("ep", "tp"),
        P("ep", None),
        P("ep", None, "tp"),
        P("ep", None, "tp"),
        P("ep", "tp", None),
    )
    return jax.shard_map(
        on_device, mesh=mesh, in_specs=in_specs, out_specs=out_specs, check_vma=False
    )
```

profile of v0, /device:TPU:9, one launch (start us, length us, event | category | flops | bytes accessed | tf_op | source)
XLA Modules:
  0.0 123.5 jit_solution(9004217932677203666)
XLA Ops:
  0.6 0.8 slice_convert_fusion
  1.4 0.8 copy.21
  2.2 0.1 eq.45
  2.4 0.3 fusion.1
  2.6 0.1 reduce_sum.48
  2.8 0.1 copy.22
  2.9 0.7 multiply_add_fusion
  3.6 0.0 copy-start.2
  3.6 0.0 copy-start.3
  3.6 0.2 select_reduce_fusion.2
  3.8 0.1 add.20
  3.9 0.6 broadcast_in_dim.78
  4.5 2.4 %convolution_convert_fusion.sent_cot = bf16[768,512]{1,0:T(8,128)(2,1)} fusion(s32[256]{0:T(256)S(1)} %bitcast.28, s32[256]{0:T(256)S(1)} %bitcast.23, bf16[256,2048]{1,0:T(8,128)(2,1)} %param.8, s32[]{:T(128)S(6)} %select_n.23), kind=kOutput, calls=%fused_computation | convolution fusion | flops 202309632 | bytes 1050628 | tf_op jit(solution)/shard_map/dot_general | solution.py:399
  6.9 0.0 copy-done.2
  6.9 0.0 copy-done.3
  6.9 2.4 %convolution_convert_fusion.1.sent_tok = bf16[768,512]{1,0:T(8,128)(2,1)} fusion(s32[256]{0:T(256)S(1)} %bitcast.29, s32[256]{0:T(256)S(1)} %bitcast.24, bf16[256,2048]{1,0:T(8,128)(2,1)} %param.7, s32[]{:T(128)S(6)} %select_n.23), kind=kOutput, calls=%fused_computation.1 | convolution fusion | flops 202309632 | bytes 1050628 | tf_op jit(solution)/shard_map/dot_general | solution.py:397
  9.3 99.9 %shard_map.110 = (bf16[768,512]{1,0:T(8,128)(2,1)}, f32[64,128]{1,0:T(8,128)}, bf16[2048,896]{1,0:T(8,128)(2,1)}, bf16[2048,896]{1,0:T(8,128)(2,1)}, bf16[896,2048]{1,0:T(8,128)(2,1)}) custom-call(bf16[768,512]{1,0:T(8,128)(2,1)} %convolution_convert_fusion.1.sent_tok, bf16[768,512]{1,0:T(8,128)(2,1)} %convolution_convert_fusion.sent_cot, ...), custom_call_target="tpu_custom_call" | custom-call | tf_op jit(solution)/shard_map/pallas_call | solution.py:416
  109.3 2.3 %convolution_convert_fusion.2 = bf16[256,512]{1,0:T(8,128)(2,1)} fusion(bf16[768,512]{1,0:T(8,128)(2,1)} %get-tuple-element.10, s32[256]{0:T(256)} %bitcast.30, s32[256]{0:T(256)} %bitcast.25), kind=kOutput, calls=%fused_computation.2 | convolution fusion | flops 202047488 | bytes 1050624 | tf_op jit(solution)/shard_map/dot_general | solution.py:460
  111.5 0.8 slice_reduce_fusion
  112.3 0.1 broadcast_in_dim.79
  112.4 1.0 select_reduce_fusion.1
  113.4 0.6 pad_maximum_fusion
  114.0 0.0 copy-start.1
  114.0 4.3 %copy.26 = bf16[1,2048,896]{2,1,0:T(8,128)(2,1)} copy(bf16[1,2048,896]{2,1,0:T(8,128)(2,1)} %bitcast.17) | data formatting | bytes 7340032
  118.3 0.0 copy-done.1
  118.3 0.0 copy-start
  118.3 1.9 %copy.27 = bf16[1,2048,896]{2,1,0:T(8,128)(2,1)} copy(bf16[1,2048,896]{2,1,0:T(8,128)(2,1)S(1)} %bitcast.16) | data formatting | bytes 7340032
  120.2 1.5 %copy-done = bf16[896,2048]{1,0:T(8,128)(2,1)S(1)} copy-done((bf16[896,2048]{1,0:T(8,128)(2,1)S(1)}, bf16[896,2048]{1,0:T(8,128)(2,1)}, u32[]{:S(2)}) %copy-start) | copy-done | bytes 3670040
  121.7 1.8 %copy.28 = bf16[1,896,2048]{2,1,0:T(8,128)(2,1)} copy(bf16[1,896,2048]{2,1,0:T(8,128)(2,1)S(1)} %bitcast.15) | data formatting | bytes 7340032
  (3 shorter events, 0.0 us)
Async XLA Ops:
  3.6 3.4 %copy-start.2 = (s32[256,1]{0,1:T(1,128)}, s32[256,1]{0,1:T(1,128)S(1)}, u32[]{:S(2)}) copy-start(s32[256,1]{0,1:T(1,128)S(1)} %get-tuple-element.17) | copy-start | bytes 3076
  3.6 3.4 %copy-start.3 = (s32[256,1]{0,1:T(1,128)}, s32[256,1]{0,1:T(1,128)S(1)}, u32[]{:S(2)}) copy-start(s32[256,1]{0,1:T(1,128)S(1)} %get-tuple-element.18) | copy-start | bytes 3076
  114.0 4.3 %copy-start.1 = (bf16[2048,896]{1,0:T(8,128)(2,1)S(1)}, bf16[2048,896]{1,0:T(8,128)(2,1)}, u32[]{:S(2)}) copy-start(bf16[2048,896]{1,0:T(8,128)(2,1)} %get-tuple-element.13) | copy-start | bytes 11010052
  118.3 3.4 %copy-start = (bf16[896,2048]{1,0:T(8,128)(2,1)S(1)}, bf16[896,2048]{1,0:T(8,128)(2,1)}, u32[]{:S(2)}) copy-start(bf16[896,2048]{1,0:T(8,128)(2,1)} %get-tuple-element.14) | copy-start | bytes 11010052
where the time goes:
time: 126 us; the launch traced here: 124 us
  Pallas kernels  99.9 us (79%)
  local copies, waits for them, and re-layouts  12.3 us (10%)
  matrix products  7.36 us (6%)
  other arithmetic  3.31 us (3%)
    pallas_call x1, Pallas kernels, on_device(): pl.pallas_call(functools.partial(expert_kernel, groups, slot, quarter), o...  99.9 us
    unnamed x12, local copies, waits for them, and re-layouts  10.3 us

commit v1 on v0

v1 whole, which is shorter than its diff:
```python
import functools

import jax
import jax.numpy as jnp
from jax import lax
from jax.experimental import pallas as pl
from jax.experimental.pallas import tpu as pltpu
from jax.sharding import PartitionSpec as P

MESH = pl.DeviceIdType.MESH
FIRST = (((0,), (0,)), ((), ()))
SUM_ROWS = 8
STAGES = 4
NEAR = 2


def expert_kernel(groups, slot, quarter,
                  routes, weights, tokens, cotangent, w_gate, w_up, w_down,
                  og, ou, od, back_rows, back_gate, places,
                  tok, cot, sent_x, sent_c, more_x, more_c, x_rows, c_rows, wg, wu, wd, wg_t, wu_t, wd_t,
                  gate_pre, up_pre, back, hidden, grads,
                  part, core_got, x_got, total, gate_all, gate_sum,
                  load_sem, first_send, first_recv, core_send, core_recv,
                  x_send, x_recv, second_send, second_recv,
                  pair_send, pair_recv, cross_send, cross_recv, home_send, home_recv,
                  sum_send, sum_recv, sumhome_send, sumhome_recv, near_sem):
    me = lax.axis_index("ep")
    t = lax.axis_index("tp")
    core = lax.rem(t, 2)
    side = t // 2
    core_peer = side * 2 + (1 - core)
    x_peer = (1 - side) * 2 + core
    x_core_peer = (1 - side) * 2 + (1 - core)
    rows = groups * slot
    ffe = wg.shape[1]
    width = wg.shape[0]
    tok_dev = tok.shape[0]
    bf, f32 = jnp.bfloat16, jnp.float32
    bits = groups.bit_length() - 1
    stages = min(STAGES, groups)
    per = groups // stages
    span = per * slot

    def flip(j):
        out = 0
        for b in range(bits):
            s = 1 << b
            out = out + s * lax.rem(lax.rem(me // s, 2) + lax.rem(j // s, 2), 2)
        return out

    def loop(lo, hi, body):
        def step(d, c):
            body(d)
            return c
        lax.fori_loop(lo, hi, step, 0)

    barrier = pltpu.get_barrier_semaphore()

    def greet(d):
        pl.semaphore_signal(barrier, inc=1, device_id=(lax.rem(me + d, groups), t),
                            device_id_type=MESH)

    loop(1, groups, greet)
    for o in range(1, 4):
        pl.semaphore_signal(barrier, inc=1, device_id=(me, lax.rem(t + o, 4)),
                            device_id_type=MESH)
    loads = [
        pltpu.make_async_copy(src, dst, load_sem.at[i])
        for i, (src, dst) in enumerate(((tokens, tok), (cotangent, cot), (w_down, wd),
                                        (w_gate, wg), (w_up, wu)))
    ]
    for load in loads:
        load.start()

    def rblk(ref, s, size=slot):
        return ref.at[pl.ds(pl.multiple_of(s * size, size if size < 16 else 16), size)]

    def cols(q):
        return pl.ds(pl.multiple_of(q * quarter, 128), quarter)

    def blk(ref, s, q):
        return ref.at[pl.ds(pl.multiple_of(s * slot, 16), slot), cols(q)]

    def rc(src, dst, ssem, rsem, ep, tp):
        return pltpu.make_async_remote_copy(
            src_ref=src, dst_ref=dst, send_sem=ssem, recv_sem=rsem,
            device_id=(ep, tp), device_id_type=MESH)

    sent = (sent_x, sent_c)
    more = (more_x, more_c)
    full = (x_rows, c_rows)

    def first(a, j):
        return rc(rblk(sent[a], j), blk(full[a], j, t), first_send.at[a, j],
                  first_recv.at[a, j], flip(j), t)

    def to_core(a, j, q):
        return rc(blk(full[a], j, q), blk(full[a], j, q), core_send.at[a, j],
                  core_recv.at[a, j], me, core_peer)

    def to_x(a, j, q):
        return rc(blk(full[a], j, q), blk(full[a], j, q), x_send.at[a, j],
                  x_recv.at[a, j], me, x_peer)

    def direct(a, j):
        return rc(rblk(more[a], j), blk(full[a], j, x_peer), x_send.at[a, j],
                  x_recv.at[a, j], flip(j), t)

    def to_core_again(a, j, q):
        return rc(blk(full[a], j, q), blk(full[a], j, q), second_send.at[a, j],
                  second_recv.at[a, j], me, core_peer)

    kinds = lax.broadcasted_iota(jnp.int32, (groups, tok_dev), 0)
    expert = jnp.bitwise_xor(kinds, me)
    hot = [(expert == routes[k:k + 1, :]).astype(f32) for k in range(2)]
    before = (lax.broadcasted_iota(jnp.int32, (tok_dev, tok_dev), 0)
              < lax.broadcasted_iota(jnp.int32, (tok_dev, tok_dev), 1)).astype(f32).astype(bf)
    earlier = jnp.dot(jnp.concatenate(hot, axis=0).astype(bf), before, preferred_element_type=f32)
    base = (kinds * slot).astype(f32)
    counts = (base + earlier[0:groups],
              base + earlier[groups:2 * groups] + jnp.sum(hot[0], axis=1, keepdims=True))
    place = [jnp.sum(hot[k] * counts[k], axis=0, keepdims=True).astype(jnp.int32)
             for k in range(2)]
    places[...] = jnp.concatenate(
        place + [jnp.full((6, tok_dev), -1, jnp.int32)], axis=0)
    share = [weights[k:k + 1, :].astype(f32) for k in range(2)]

    def picks(j):
        at = lax.broadcasted_iota(jnp.int32, (slot, tok_dev), 0) + j * slot
        hit = [at == places[k:k + 1, :] for k in range(2)]
        plain = jnp.where(hit[0] | hit[1], 1.0, 0.0).astype(bf)
        scaled = (jnp.where(hit[0], share[0], 0.0) + jnp.where(hit[1], share[1], 0.0)).astype(bf)
        return plain, scaled

    pl.semaphore_wait(barrier, groups + 2)
    loads[0].wait()
    loads[1].wait()

    def dispatch(j):
        plain, scaled = picks(j)
        r = pl.ds(pl.multiple_of(j * slot, 16), slot)
        sent_x[r, :] = jnp.dot(plain, tok[:, cols(t)], preferred_element_type=f32).astype(bf)
        first(0, j).start()
        sent_c[r, :] = jnp.dot(scaled, cot[:, cols(t)], preferred_element_type=f32).astype(bf)
        first(1, j).start()

    def dispatch_more(j):
        plain, scaled = picks(j)
        r = pl.ds(pl.multiple_of(j * slot, 16), slot)
        more_x[r, :] = jnp.dot(plain, tok[:, cols(x_peer)], preferred_element_type=f32).astype(bf)
        direct(0, j).start()
        more_c[r, :] = jnp.dot(scaled, cot[:, cols(x_peer)], preferred_element_type=f32).astype(bf)
        direct(1, j).start()

    near = min(NEAR, groups)
    loop(1, min(2 * per, groups), dispatch)
    loop(1, near, dispatch_more)
    loop(min(2 * per, groups), groups, dispatch)
    plain, scaled = picks(0)
    x_rows[0:slot, :] = jnp.dot(plain, tok[...], preferred_element_type=f32).astype(bf)
    c_rows[0:slot, :] = jnp.dot(scaled, cot[...], preferred_element_type=f32).astype(bf)

    def blocks(g):
        return max(1, g * per), (g + 1) * per

    def arrive(a, j):
        first(a, j).wait_recv()
        to_x(a, j, t).start()
        to_core(a, j, t).start()

    def arrive_near(a, j):
        first(a, j).wait_recv()
        to_core(a, j, t).start()

    def relay(a, j):
        to_x(a, j, x_peer).wait_recv()
        to_core_again(a, j, x_peer).start()

    def settled(a, j):
        to_core(a, j, core_peer).wait_recv()
        to_core_again(a, j, x_core_peer).wait_recv()

    def each(k, fn):
        lo, hi = max(1, k * per // 2), (k + 1) * per // 2

        def run(lo, hi, fn):
            def body(j):
                fn(0, j)
                fn(1, j)
            if hi > lo:
                loop(lo, hi, body)
        if fn is arrive:
            run(lo, min(hi, near), arrive_near)
            lo = max(lo, near)
        run(lo, hi, fn)

    def turn(src, dst):
        for lo in range(0, src.shape[0], 128):
            n = min(128, src.shape[0] - lo)
            dst[:, lo:lo + n] = src[lo:lo + n, :].T

    def forward(g):
        r = slice(g * span, (g + 1) * span)
        gate_pre[...] = jnp.dot(x_rows[r, :], wg[...], preferred_element_type=f32)
        up_pre[...] = jnp.dot(x_rows[r, :], wu[...], preferred_element_type=f32)

    def backward(g):
        r = slice(g * span, (g + 1) * span)
        back[...] = jnp.dot(c_rows[r, :], wd_t[...], preferred_element_type=f32)

    lanes = gate_all.shape[2]

    def elementwise(g):
        def body(i):
            r = pl.ds(pl.multiple_of(i * slot, 16), slot)
            w = pl.ds(pl.multiple_of((g * per + i) * slot, 16), slot)
            summed = jnp.zeros((slot, 128), f32)
            for lo in range(0, ffe, 128):
                v = gate_pre[r, lo:lo + 128]
                u = up_pre[r, lo:lo + 128]
                b = back[r, lo:lo + 128]
                logistic = jax.nn.sigmoid(v)
                act = v * logistic
                h = (act * u).astype(bf)
                hidden[w, lo:lo + 128] = h
                summed = summed + h.astype(f32) * b
                grads[w, lo:lo + 128] = (b * u * logistic * (1.0 + v * (1.0 - logistic))).astype(bf)
                grads[w, ffe + lo:ffe + lo + 128] = (b * act).astype(bf)
            if lanes > slot:
                summed = jnp.concatenate([summed, jnp.zeros((lanes - slot, 128), f32)], axis=0)
            row = jnp.sum(summed.T, axis=0, keepdims=True)
            s = pl.ds(pl.multiple_of((g * per + i) * SUM_ROWS, SUM_ROWS), SUM_ROWS)
            gate_all[t, s, :] = jnp.broadcast_to(row, (SUM_ROWS, lanes))
        loop(0, per, body)

    def row_product(g, q, i):
        r = slice(g * span, (g + 1) * span)
        value = jnp.dot(grads[r, 0:ffe], wg_t[:, cols(q)], preferred_element_type=f32)
        value = value + jnp.dot(grads[r, ffe:2 * ffe], wu_t[:, cols(q)],
                                preferred_element_type=f32)
        part[i, r, :] = value.astype(bf)

    def pair(g, i):
        r = pl.ds(g * span, span)
        return rc(part.at[i, r], core_got.at[i, r], pair_send.at[i, g], pair_recv.at[i, g],
                  me, core_peer)

    def cross(s):
        return rc(rblk(part.at[2], s), rblk(x_got, s), cross_send.at[s], cross_recv.at[s],
                  me, x_peer)

    def home(j):
        return rc(rblk(total, j), rblk(back_rows, j), home_send.at[j], home_recv.at[j],
                  flip(j), t)

    def give_back(g):
        row_product(g, x_core_peer, 0)
        pair(g, 0).start()
        row_product(g, x_peer, 2)
        pair(g, 0).wait_recv()

        def add_cross(s):
            r = pl.ds(pl.multiple_of(s * slot, 16), slot)
            part[2, r, :] = (part[2, r, :].astype(f32) + core_got[0, r, :].astype(f32)).astype(bf)
            cross(s).start()
        loop(g * per, (g + 1) * per, add_cross)
        row_product(g, core_peer, 1)
        pair(g, 1).start()
        row_product(g, t, 3)

    def finish(g):
        pair(g, 1).wait_recv()

        def sum_of(s):
            r = pl.ds(pl.multiple_of(s * slot, 16), slot)
            cross(s).wait_recv()
            return r, (part[3, r, :].astype(f32) + core_got[1, r, :].astype(f32)
                       + x_got[r, :].astype(f32)).astype(bf)

        def body(s):
            r, value = sum_of(s)
            total[r, :] = value
            home(s).start()
        if g == 0:
            r, value = sum_of(0)
            back_rows[r, :] = value
        lo, hi = blocks(g)
        if hi > lo:
            loop(lo, hi, body)

    half = rows // 2

    def x_grads(h, lo, hi):
        r = slice(h * half, (h + 1) * half)

        def body(i):
            m = pl.ds(pl.multiple_of(i * 256, 256), 256)
            left = x_rows[r, m]
            for out, at in ((og, 0), (ou, ffe)):
                value = lax.dot_general(left, grads[r, at:at + ffe], FIRST,
                                        preferred_element_type=f32)
                if h:
                    value = value + out[m, :].astype(f32)
                out[m, :] = value.astype(bf)
        loop(lo, hi, body)

    def down_grads(h):
        r = slice(h * half, (h + 1) * half)
        for lo in range(0, ffe, 256):
            n = min(256, ffe - lo)
            value = lax.dot_general(hidden[r, lo:lo + n], c_rows[r, :], FIRST,
                                    preferred_element_type=f32)
            if h:
                value = value + od[lo:lo + n, :].astype(f32)
            od[lo:lo + n, :] = value.astype(bf)

    x_steps = width // 256
    loads[2].wait()
    each(0, arrive)
    each(1, arrive)
    turn(wd, wd_t)
    loads[3].wait()
    turn(wg, wg_t)
    loads[4].wait()
    turn(wu, wu_t)
    each(2, arrive)
    each(3, arrive)
    each(0, relay)
    each(1, relay)
    each(0, settled)
    each(1, settled)
    forward(0)
    backward(0)
    elementwise(0)
    each(4, arrive)
    each(2, relay)
    give_back(0)
    each(3, relay)
    each(5, arrive)
    each(2, settled)
    each(3, settled)
    forward(1)
    backward(1)
    elementwise(1)
    each(4, relay)
    give_back(1)
    x_grads(0, 0, x_steps // 2)
    each(6, arrive)
    each(5, relay)
    each(4, settled)
    each(5, settled)
    forward(2)
    each(7, arrive)
    backward(2)
    elementwise(2)
    give_back(2)
    finish(0)
    each(6, relay)
    x_grads(0, x_steps // 2, x_steps)
    each(7, relay)
    finish(1)
    down_grads(0)
    each(6, settled)
    each(7, settled)
    forward(3)
    backward(3)
    elementwise(3)
    sums = [rc(gate_all.at[t], gate_all.at[t], sum_send.at[o - 1], sum_recv.at[o - 1],
               me, lax.rem(t + o, 4)) for o in range(1, 4)]
    for copy in sums:
        copy.start()
    finish(2)
    give_back(3)
    x_grads(1, 0, x_steps // 2)
    for copy in sums:
        copy.wait_recv()
    gate_sum[...] = (gate_all[0] + gate_all[1]) + (gate_all[2] + gate_all[3])

    def sum_home(j):
        return rc(rblk(gate_sum, j, SUM_ROWS), rblk(back_gate, j, SUM_ROWS),
                  sumhome_send.at[j], sumhome_recv.at[j], flip(j), t)

    loop(1, groups, lambda j: sum_home(j).start())
    back_gate[0:SUM_ROWS, :] = gate_sum[0:SUM_ROWS, :]
    finish(3)
    x_grads(1, x_steps // 2, x_steps)
    down_grads(1)

    def landed(j):
        sum_home(j).wait_recv()
        home(j).wait_recv()

    def drain(j):
        for a in range(2):
            first(a, j).wait_send()
            to_core(a, j, t).wait_send()
            to_x(a, j, t).wait_send()
            to_core_again(a, j, x_peer).wait_send()
        sum_home(j).wait_send()
        home(j).wait_send()

    loop(1, groups, landed)
    loop(1, groups, drain)
    loop(0, groups, lambda s: cross(s).wait_send())
    for g in range(stages):
        for i in range(2):
            pair(g, i).wait_send()
    for copy in sums:
        copy.wait_send()


def collect_kernel(groups, slot, places, weights, back_rows, back_gate, og, ou, od,
                   grad_tokens, grad_gates, out_gate, out_up, out_down, out_sem):
    bf, f32 = jnp.bfloat16, jnp.float32
    outs = []
    for i, (src, dst) in enumerate(((og, out_gate), (ou, out_up), (od, out_down))):
        step = src.shape[0] // 2
        for h in range(2):
            copy = pltpu.make_async_copy(src.at[h * step:(h + 1) * step],
                                         dst.at[h * step:(h + 1) * step], out_sem.at[i, h])
            copy.start()
            outs.append(copy)
    tok_dev = places.shape[1]
    rows = groups * slot
    lanes = back_gate.shape[1]
    at = lax.broadcasted_iota(jnp.int32, (rows, tok_dev), 0)
    hit = (at == places[0:1, :]) | (at == places[1:2, :])
    grad_tokens[...] = lax.dot_general(
        jnp.where(hit, 1.0, 0.0).astype(bf), back_rows[...], FIRST,
        preferred_element_type=f32).astype(bf)
    sums = [jnp.zeros((1, tok_dev), f32), jnp.zeros((1, tok_dev), f32)]
    for j in range(groups):
        row = back_gate[j * SUM_ROWS:j * SUM_ROWS + 1, :]
        column = jnp.broadcast_to(row, (lanes, lanes)).T[0:slot, 0:1]
        here = lax.broadcasted_iota(jnp.int32, (slot, tok_dev), 0) + j * slot
        for k in range(2):
            sums[k] = sums[k] + jnp.sum(
                jnp.where(here == places[k:k + 1, :], column, 0.0), axis=0, keepdims=True)
    grad_gates[...] = jnp.concatenate(sums, axis=0) / weights[...].astype(f32)
    for copy in outs:
        copy.wait()


def on_device(tokens, cotangent, gate_weights, routes, w_gate, w_up, w_down):
    tok_dev, width = tokens.shape
    top_k = routes.shape[1]
    groups = lax.axis_size("ep")
    narrow = lax.axis_size("tp")
    capacity = 3 * top_k * tok_dev // (2 * groups)
    slot = -(-capacity // 16) * 16
    quarter = width // narrow
    ffe = w_gate.shape[2]
    rows = groups * slot
    lanes = -(-slot // 128) * 128
    stages = min(STAGES, groups)
    span = rows // stages
    vmem = pl.BlockSpec(memory_space=pltpu.VMEM)
    hbm = pl.BlockSpec(memory_space=pl.ANY)
    bf, f32 = jnp.bfloat16, jnp.float32
    dma = pltpu.SemaphoreType.DMA
    per = dma((groups,))
    twice = dma((2, groups))
    routes_t = routes.T
    weights_t = gate_weights.T
    og, ou, od, back_rows, back_gate, places = pl.pallas_call(
        functools.partial(expert_kernel, groups, slot, quarter),
        out_shape=(
            pltpu.VMEM((width, ffe), bf),
            pltpu.VMEM((width, ffe), bf),
            pltpu.VMEM((ffe, width), bf),
            pltpu.VMEM((rows, quarter), bf),
            pltpu.VMEM((groups * SUM_ROWS, lanes), f32),
            pltpu.VMEM((8, tok_dev), jnp.int32),
        ),
        in_specs=[vmem, vmem, hbm, hbm, hbm, hbm, hbm],
        out_specs=(vmem,) * 6,
        scratch_shapes=[
            pltpu.VMEM((tok_dev, width), bf),
            pltpu.VMEM((tok_dev, width), bf),
            pltpu.VMEM((rows, quarter), bf),
            pltpu.VMEM((rows, quarter), bf),
            pltpu.VMEM((min(NEAR, groups) * slot, quarter), bf),
            pltpu.VMEM((min(NEAR, groups) * slot, quarter), bf),
            pltpu.VMEM((rows, width), bf),
            pltpu.VMEM((rows, width), bf),
            pltpu.VMEM((width, ffe), bf),
            pltpu.VMEM((width, ffe), bf),
            pltpu.VMEM((ffe, width), bf),
            pltpu.VMEM((ffe, width), bf),
            pltpu.VMEM((ffe, width), bf),
            pltpu.VMEM((width, ffe), bf),
            pltpu.VMEM((span, ffe), f32),
            pltpu.VMEM((span, ffe), f32),
            pltpu.VMEM((span, ffe), f32),
            pltpu.VMEM((rows, ffe), bf),
            pltpu.VMEM((rows, 2 * ffe), bf),
            pltpu.VMEM((4, rows, quarter), bf),
            pltpu.VMEM((2, rows, quarter), bf),
            pltpu.VMEM((rows, quarter), bf),
            pltpu.VMEM((rows, quarter), bf),
            pltpu.VMEM((4, groups * SUM_ROWS, lanes), f32),
            pltpu.VMEM((groups * SUM_ROWS, lanes), f32),
            dma((5,)),
            twice, twice, twice, twice, twice, twice, twice, twice,
            dma((2, stages)), dma((2, stages)),
            per, per, per, per,
            dma((3,)), dma((3,)),
            per, per,
            dma((3,)),
        ],
        compiler_params=pltpu.CompilerParams(
            collective_id=0, has_side_effects=True, vmem_limit_bytes=52 * 2 ** 20),
        name="expert",
    )(routes_t, weights_t, tokens, cotangent, w_gate[0], w_up[0], w_down[0])
    held = [pltpu.with_memory_space_constraint(x, pltpu.VMEM)
            for x in (places, back_rows, back_gate, og, ou, od)]
    grad_tokens, grad_gates, grad_gate_w, grad_up_w, grad_down = pl.pallas_call(
        functools.partial(collect_kernel, groups, slot),
        out_shape=(
            jax.ShapeDtypeStruct((tok_dev, quarter), bf),
            jax.ShapeDtypeStruct((top_k, tok_dev), f32),
            jax.ShapeDtypeStruct((width, ffe), bf),
            jax.ShapeDtypeStruct((width, ffe), bf),
            jax.ShapeDtypeStruct((ffe, width), bf),
        ),
        in_specs=[vmem] * 7,
        out_specs=(vmem, vmem, hbm, hbm, hbm),
        scratch_shapes=[dma((3, 2))],
        compiler_params=pltpu.CompilerParams(vmem_limit_bytes=8 * 2 ** 20),
        name="collect",
    )(held[0], weights_t, *held[1:])
    return (grad_tokens, grad_gates.T, grad_gate_w[None], grad_up_w[None], grad_down[None])


def solution(mesh):
    in_specs = (
        P("ep", None),
        P("ep", None),
        P("ep", None),
        P("ep", None),
        P("ep", None, "tp"),
        P("ep", None, "tp"),
        P("ep", "tp", None),
    )
    out_specs = (
        P("ep", "tp"),
        P("ep", None),
        P("ep", None, "tp"),
        P("ep", None, "tp"),
        P("ep", "tp", None),
    )
    return jax.shard_map(
        on_device, mesh=mesh, in_specs=in_specs, out_specs=out_specs, check_vma=False
    )
```

time: 126 us -> 84.8 us (0.67); the launches traced: 124 us -> 84.7 us
  Pallas kernels: 99.9 us -> 83.8 us
  local copies, waits for them, and re-layouts: 12.3 us -> 0.01 us
  matrix products: 7.36 us -> 0 us
  other arithmetic: 3.31 us -> 0 us
    pallas_call x1, Pallas kernels: 99.9 us -> 78.8 us  [on_device(): pl.pallas_call(functools.partial(expert_kernel, groups, slot, quarter), o...]
    unnamed x12 -> x2, local copies, waits for them, and re-layouts: 10.3 us -> 0.01 us
    dot_general x4 -> x0, matrix products: 7.36 us -> none  [the longest x1 2.4 us: on_device(): lax.dot_general(select, tok_part, contract_first, preferred_element_type=...]
    pallas_call x0 -> x1, Pallas kernels: none -> 5.02 us  [on_device(): pl.pallas_call(functools.partial(collect_kernel, groups, slot), out_shape...]
where the time goes in v1:
time: 84.8 us; the launch traced here: 84.7 us
  Pallas kernels  83.8 us (99%)
    pallas_call x1, Pallas kernels, on_device(): pl.pallas_call(functools.partial(expert_kernel, groups, slot, quarter), o...  78.8 us
    pallas_call x1, Pallas kernels, on_device(): pl.pallas_call(functools.partial(collect_kernel, groups, slot), out_shape...  5.02 us

profile of v1, /device:TPU:9, one launch (start us, length us, event | category | flops | bytes accessed | tf_op | source)
XLA Modules:
  0.0 84.7 jit_solution(7518276035888490688)
XLA Ops:
  0.6 0.0 copy-start
  0.6 78.8 %expert.1 = (bf16[2048,896]{1,0:T(8,128)(2,1)S(1)}, bf16[2048,896]{1,0:T(8,128)(2,1)S(1)}, bf16[896,2048]{1,0:T(8,128)(2,1)S(1)}, bf16[768,512]{1,0:T(8,128)(2,1...) custom-call(s32[2,256]{1,0:T(2,128)} %bitcast.14, bf16[2,256]{1,0:T(2,128)(2,1)} %bitcast.9, ...), custom_call_target="tpu_custom_call" | custom-call | tf_op jit(solution)/shard_map/expert/pallas_call | solution.py:465
  79.4 0.0 copy-done
  79.5 5.0 %collect.1 = (bf16[256,512]{1,0:T(8,128)(2,1)}, f32[2,256]{1,0:T(2,128)}, bf16[2048,896]{1,0:T(8,128)(2,1)}, bf16[2048,896]{1,0:T(8,128)(2,1)}, bf16[896,2048]{1,0:T(8,128)(2,1)}) custom-call(s32[8,256]{1,0:T(8,128)S(1)} %get-tuple-element.16.places, bf16[2,256]{1,0:T(2,128)(2,1)S(1)} %bitcast.10, bf16[768,512]{1,0:T(8,128)(2,1)S(1)} %get-tuple-element.17.back_rows, ...), custom_call_target="tpu_custom_call" | custom-call | tf_op jit(solution)/shard_map/collect/pallas_call | solution.py:517
Async XLA Ops:
  0.6 78.8 %copy-start = (bf16[256,2]{0,1:T(2,128)(2,1)S(1)}, bf16[256,2]{0,1:T(2,128)(2,1)}, u32[]{:S(2)}) copy-start(bf16[256,2]{0,1:T(2,128)(2,1)} %param.9) | copy-start | bytes 3076

commit v2 on v1

--- a/solution.py
+++ b/solution.py
@@ -10,15 +10,15 @@
 MESH = pl.DeviceIdType.MESH
 FIRST = (((0,), (0,)), ((), ()))
 SUM_ROWS = 8
-STAGES = 4
-NEAR = 2
+EIGHTHS = (0, 2, 4, 6, 8)
+DIRECT = (2, 3)
 
 
 def expert_kernel(groups, slot, quarter,
                   routes, weights, tokens, cotangent, w_gate, w_up, w_down,
-                  og, ou, od, back_rows, back_gate, places,
-                  tok, cot, sent_x, sent_c, more_x, more_c, x_rows, c_rows, wg, wu, wd, wg_t, wu_t, wd_t,
-                  gate_pre, up_pre, back, hidden, grads,
+                  og, ou, od, back_rows, back_gate, places, hidden, c_rows,
+                  tok, cot, sent_x, sent_c, more_x, more_c, x_rows, wg, wu, wd, wg_t, wu_t, wd_t,
+                  gate_pre, up_pre, back, grads,
                   part, core_got, x_got, total, gate_all, gate_sum,
                   load_sem, first_send, first_recv, core_send, core_recv,
                   x_send, x_recv, second_send, second_recv,
@@ -37,9 +37,14 @@
     tok_dev = tok.shape[0]
     bf, f32 = jnp.bfloat16, jnp.float32
     bits = groups.bit_length() - 1
-    stages = min(STAGES, groups)
-    per = groups // stages
-    span = per * slot
+    stages = len(EIGHTHS) - 1
+    edges = [e * groups // 8 for e in EIGHTHS]
+
+    def rows_of(g):
+        return slice(edges[g] * slot, edges[g + 1] * slot)
+
+    def size_of(g):
+        return (edges[g + 1] - edges[g]) * slot
 
     def flip(j):
         out = 0
@@ -86,6 +91,10 @@
             src_ref=src, dst_ref=dst, send_sem=ssem, recv_sem=rsem,
             device_id=(ep, tp), device_id_type=MESH)
 
+    is_end = 1 - (lax.rem(me // max(1, groups // 4), 3) + 1) // 2
+    outer = is_end == 1
+    inner = is_end == 0
+
     sent = (sent_x, sent_c)
     more = (more_x, more_c)
     full = (x_rows, c_rows)
@@ -103,7 +112,7 @@
                   x_recv.at[a, j], me, x_peer)
 
     def direct(a, j):
-        return rc(rblk(more[a], j), blk(full[a], j, x_peer), x_send.at[a, j],
+        return rc(rblk(more[a], j - begin), blk(full[a], j, x_peer), x_send.at[a, j],
                   x_recv.at[a, j], flip(j), t)
 
     def to_core_again(a, j, q):
@@ -144,31 +153,37 @@
         sent_c[r, :] = jnp.dot(scaled, cot[:, cols(t)], preferred_element_type=f32).astype(bf)
         first(1, j).start()
 
+    begin, end = DIRECT
+
     def dispatch_more(j):
         plain, scaled = picks(j)
-        r = pl.ds(pl.multiple_of(j * slot, 16), slot)
+        r = pl.ds(pl.multiple_of((j - begin) * slot, 16), slot)
         more_x[r, :] = jnp.dot(plain, tok[:, cols(x_peer)], preferred_element_type=f32).astype(bf)
         direct(0, j).start()
         more_c[r, :] = jnp.dot(scaled, cot[:, cols(x_peer)], preferred_element_type=f32).astype(bf)
         direct(1, j).start()
 
-    near = min(NEAR, groups)
-    loop(1, min(2 * per, groups), dispatch)
-    loop(1, near, dispatch_more)
-    loop(min(2 * per, groups), groups, dispatch)
+    far = edges[2]
+
+    @pl.when(inner)
+    def _():
+        dispatch(far)
+    loop(1, far, dispatch)
+    loop(begin, end, dispatch_more)
+    loop(far + (1 - is_end), groups, dispatch)
     plain, scaled = picks(0)
     x_rows[0:slot, :] = jnp.dot(plain, tok[...], preferred_element_type=f32).astype(bf)
     c_rows[0:slot, :] = jnp.dot(scaled, cot[...], preferred_element_type=f32).astype(bf)
 
     def blocks(g):
-        return max(1, g * per), (g + 1) * per
+        return max(1, edges[g]), edges[g + 1]
 
     def arrive(a, j):
         first(a, j).wait_recv()
         to_x(a, j, t).start()
         to_core(a, j, t).start()
 
-    def arrive_near(a, j):
+    def arrive_direct(a, j):
         first(a, j).wait_recv()
         to_core(a, j, t).start()
 
@@ -180,19 +195,23 @@
         to_core(a, j, core_peer).wait_recv()
         to_core_again(a, j, x_core_peer).wait_recv()
 
-    def each(k, fn):
-        lo, hi = max(1, k * per // 2), (k + 1) * per // 2
-
-        def run(lo, hi, fn):
-            def body(j):
-                fn(0, j)
-                fn(1, j)
-            if hi > lo:
-                loop(lo, hi, body)
+    def span_of(k):
+        return max(1, k * groups // 8), (k + 1) * groups // 8
+
+    def run(lo, hi, fn, tensors):
+        def body(j):
+            for a in tensors:
+                fn(a, j)
+        if hi > lo:
+            loop(lo, hi, body)
+
+    def each(k, fn, tensors=(0, 1)):
+        lo, hi = span_of(k)
         if fn is arrive:
-            run(lo, min(hi, near), arrive_near)
-            lo = max(lo, near)
-        run(lo, hi, fn)
+            run(lo, min(hi, begin), arrive, tensors)
+            run(max(lo, begin), min(hi, end), arrive_direct, tensors)
+            lo = max(lo, end)
+        run(lo, hi, fn, tensors)
 
     def turn(src, dst):
         for lo in range(0, src.shape[0], 128):
@@ -200,20 +219,20 @@
             dst[:, lo:lo + n] = src[lo:lo + n, :].T
 
     def forward(g):
-        r = slice(g * span, (g + 1) * span)
-        gate_pre[...] = jnp.dot(x_rows[r, :], wg[...], preferred_element_type=f32)
-        up_pre[...] = jnp.dot(x_rows[r, :], wu[...], preferred_element_type=f32)
+        r, n = rows_of(g), size_of(g)
+        gate_pre[0:n, :] = jnp.dot(x_rows[r, :], wg[...], preferred_element_type=f32)
+        up_pre[0:n, :] = jnp.dot(x_rows[r, :], wu[...], preferred_element_type=f32)
 
     def backward(g):
-        r = slice(g * span, (g + 1) * span)
-        back[...] = jnp.dot(c_rows[r, :], wd_t[...], preferred_element_type=f32)
+        r, n = rows_of(g), size_of(g)
+        back[0:n, :] = jnp.dot(c_rows[r, :], wd_t[...], preferred_element_type=f32)
 
     lanes = gate_all.shape[2]
 
     def elementwise(g):
         def body(i):
             r = pl.ds(pl.multiple_of(i * slot, 16), slot)
-            w = pl.ds(pl.multiple_of((g * per + i) * slot, 16), slot)
+            w = pl.ds(pl.multiple_of((edges[g] + i) * slot, 16), slot)
             summed = jnp.zeros((slot, 128), f32)
             for lo in range(0, ffe, 128):
                 v = gate_pre[r, lo:lo + 128]
@@ -229,19 +248,18 @@
             if lanes > slot:
                 summed = jnp.concatenate([summed, jnp.zeros((lanes - slot, 128), f32)], axis=0)
             row = jnp.sum(summed.T, axis=0, keepdims=True)
-            s = pl.ds(pl.multiple_of((g * per + i) * SUM_ROWS, SUM_ROWS), SUM_ROWS)
-            gate_all[t, s, :] = jnp.broadcast_to(row, (SUM_ROWS, lanes))
-        loop(0, per, body)
+            gate_all[t, pl.ds(edges[g] + i, 1), :] = row
+        loop(0, edges[g + 1] - edges[g], body)
 
     def row_product(g, q, i):
-        r = slice(g * span, (g + 1) * span)
+        r = rows_of(g)
         value = jnp.dot(grads[r, 0:ffe], wg_t[:, cols(q)], preferred_element_type=f32)
         value = value + jnp.dot(grads[r, ffe:2 * ffe], wu_t[:, cols(q)],
                                 preferred_element_type=f32)
         part[i, r, :] = value.astype(bf)
 
     def pair(g, i):
-        r = pl.ds(g * span, span)
+        r = pl.ds(edges[g] * slot, size_of(g))
         return rc(part.at[i, r], core_got.at[i, r], pair_send.at[i, g], pair_recv.at[i, g],
                   me, core_peer)
 
@@ -252,18 +270,29 @@
     def home(j):
         return rc(rblk(total, j), rblk(back_rows, j), home_send.at[j], home_recv.at[j],
                   flip(j), t)
+
+    def products(g):
+        row_product(g, x_core_peer, 0)
+        pair(g, 0).start()
+        row_product(g, x_peer, 2)
+        row_product(g, core_peer, 1)
+        pair(g, 1).start()
+        row_product(g, t, 3)
+
+    def crosses(g):
+        pair(g, 0).wait_recv()
+
+        def add_cross(s):
+            r = pl.ds(pl.multiple_of(s * slot, 16), slot)
+            part[2, r, :] = (part[2, r, :].astype(f32) + core_got[0, r, :].astype(f32)).astype(bf)
+            cross(s).start()
+        loop(0, edges[g + 1] - edges[g], lambda i: add_cross(edges[g + 1] - 1 - i))
 
     def give_back(g):
         row_product(g, x_core_peer, 0)
         pair(g, 0).start()
         row_product(g, x_peer, 2)
-        pair(g, 0).wait_recv()
-
-        def add_cross(s):
-            r = pl.ds(pl.multiple_of(s * slot, 16), slot)
-            part[2, r, :] = (part[2, r, :].astype(f32) + core_got[0, r, :].astype(f32)).astype(bf)
-            cross(s).start()
-        loop(g * per, (g + 1) * per, add_cross)
+        crosses(g)
         row_product(g, core_peer, 1)
         pair(g, 1).start()
         row_product(g, t, 3)
@@ -281,38 +310,32 @@
             r, value = sum_of(s)
             total[r, :] = value
             home(s).start()
+        lo, hi = blocks(g)
+        if hi > lo:
+            loop(lo, hi, body)
         if g == 0:
             r, value = sum_of(0)
             back_rows[r, :] = value
-        lo, hi = blocks(g)
-        if hi > lo:
-            loop(lo, hi, body)
-
-    half = rows // 2
-
-    def x_grads(h, lo, hi):
-        r = slice(h * half, (h + 1) * half)
-
+
+    def x_grads(lo, hi):
         def body(i):
             m = pl.ds(pl.multiple_of(i * 256, 256), 256)
-            left = x_rows[r, m]
-            for out, at in ((og, 0), (ou, ffe)):
-                value = lax.dot_general(left, grads[r, at:at + ffe], FIRST,
-                                        preferred_element_type=f32)
-                if h:
-                    value = value + out[m, :].astype(f32)
-                out[m, :] = value.astype(bf)
+            left = x_rows[:, m]
+            og[m, :] = lax.dot_general(left, grads[:, 0:ffe], FIRST,
+                                       preferred_element_type=f32).astype(bf)
+            ou[m, :] = lax.dot_general(left, grads[:, ffe:2 * ffe], FIRST,
+                                       preferred_element_type=f32).astype(bf)
         loop(lo, hi, body)
 
-    def down_grads(h):
-        r = slice(h * half, (h + 1) * half)
+    half = rows // 2
+
+    def down_grads():
         for lo in range(0, ffe, 256):
             n = min(256, ffe - lo)
-            value = lax.dot_general(hidden[r, lo:lo + n], c_rows[r, :], FIRST,
-                                    preferred_element_type=f32)
-            if h:
-                value = value + od[lo:lo + n, :].astype(f32)
-            od[lo:lo + n, :] = value.astype(bf)
+            od[lo:lo + n, :] = lax.dot_general(
+                hidden[0:half, lo:lo + n], c_rows[0:half, :], FIRST,
+                preferred_element_type=f32).astype(bf)
+
 
     x_steps = width // 256
     loads[2].wait()
@@ -323,8 +346,6 @@
     turn(wg, wg_t)
     loads[4].wait()
     turn(wu, wu_t)
-    each(2, arrive)
-    each(3, arrive)
     each(0, relay)
     each(1, relay)
     each(0, settled)
@@ -332,37 +353,66 @@
     forward(0)
     backward(0)
     elementwise(0)
+
+    @pl.when(inner)
+    def _():
+        each(2, arrive)
+        each(3, arrive)
+    products(0)
+
+    @pl.when(outer)
+    def _():
+        crosses(0)
+        each(2, arrive)
+        each(3, arrive)
     each(4, arrive)
+
+    @pl.when(inner)
+    def _():
+        crosses(0)
     each(2, relay)
-    give_back(0)
+
+    @pl.when(outer)
+    def _():
+        each(5, arrive)
     each(3, relay)
-    each(5, arrive)
     each(2, settled)
     each(3, settled)
     forward(1)
+
+    @pl.when(inner)
+    def _():
+        each(5, arrive)
     backward(1)
     elementwise(1)
     each(4, relay)
-    give_back(1)
-    x_grads(0, 0, x_steps // 2)
+    products(1)
     each(6, arrive)
+
+    @pl.when(outer)
+    def _():
+        each(7, arrive)
     each(5, relay)
     each(4, settled)
     each(5, settled)
     forward(2)
-    each(7, arrive)
     backward(2)
     elementwise(2)
+
+    @pl.when(inner)
+    def _():
+        each(7, arrive)
     give_back(2)
+    crosses(1)
     finish(0)
     each(6, relay)
-    x_grads(0, x_steps // 2, x_steps)
-    each(7, relay)
-    finish(1)
-    down_grads(0)
+    each(7, relay, (0,))
+    down_grads()
     each(6, settled)
-    each(7, settled)
+    each(7, settled, (0,))
     forward(3)
+    each(7, relay, (1,))
+    each(7, settled, (1,))
     backward(3)
     elementwise(3)
     sums = [rc(gate_all.at[t], gate_all.at[t], sum_send.at[o - 1], sum_recv.at[o - 1],
@@ -371,10 +421,14 @@
         copy.start()
     finish(2)
     give_back(3)
-    x_grads(1, 0, x_steps // 2)
+    finish(1)
+    x_grads(0, x_steps // 4)
     for copy in sums:
         copy.wait_recv()
-    gate_sum[...] = (gate_all[0] + gate_all[1]) + (gate_all[2] + gate_all[3])
+    gate_rows = (gate_all[0] + gate_all[1]) + (gate_all[2] + gate_all[3])
+    for j in range(groups):
+        gate_sum[j * SUM_ROWS:(j + 1) * SUM_ROWS, :] = jnp.broadcast_to(
+            gate_rows[j:j + 1, :], (SUM_ROWS, lanes))
 
     def sum_home(j):
         return rc(rblk(gate_sum, j, SUM_ROWS), rblk(back_gate, j, SUM_ROWS),
@@ -382,9 +436,9 @@
 
     loop(1, groups, lambda j: sum_home(j).start())
     back_gate[0:SUM_ROWS, :] = gate_sum[0:SUM_ROWS, :]
+    x_grads(x_steps // 4, x_steps // 2)
     finish(3)
-    x_grads(1, x_steps // 2, x_steps)
-    down_grads(1)
+    x_grads(x_steps // 2, x_steps)
 
     def landed(j):
         sum_home(j).wait_recv()
@@ -409,17 +463,29 @@
         copy.wait_send()
 
 
-def collect_kernel(groups, slot, places, weights, back_rows, back_gate, og, ou, od,
-                   grad_tokens, grad_gates, out_gate, out_up, out_down, out_sem):
+def collect_kernel(groups, slot, places, weights, back_rows, back_gate, hidden, c_rows, og, ou, od,
+                   grad_tokens, grad_gates, out_gate, out_up, out_down, summed, out_sem):
     bf, f32 = jnp.bfloat16, jnp.float32
     outs = []
-    for i, (src, dst) in enumerate(((og, out_gate), (ou, out_up), (od, out_down))):
-        step = src.shape[0] // 2
-        for h in range(2):
-            copy = pltpu.make_async_copy(src.at[h * step:(h + 1) * step],
-                                         dst.at[h * step:(h + 1) * step], out_sem.at[i, h])
-            copy.start()
-            outs.append(copy)
+
+    def put(src, dst, i, h, lo, n):
+        copy = pltpu.make_async_copy(src.at[lo:lo + n], dst.at[lo:lo + n], out_sem.at[i, h])
+        copy.start()
+        outs.append(copy)
+
+    for i, (src, dst) in enumerate(((og, out_gate), (ou, out_up))):
+        step = src.shape[0] // 4
+        for h in range(4):
+            put(src, dst, i, h, h * step, step)
+    half = groups * slot // 2
+    ffe = hidden.shape[1]
+    step = -(-ffe // 4 // 128) * 128
+    for h, lo in enumerate(range(0, ffe, step)):
+        n = min(step, ffe - lo)
+        value = lax.dot_general(hidden[half:, lo:lo + n], c_rows[half:, :], FIRST,
+                                preferred_element_type=f32)
+        summed[lo:lo + n, :] = (value + od[lo:lo + n, :].astype(f32)).astype(bf)
+        put(summed, out_down, 2, h, lo, n)
     tok_dev = places.shape[1]
     rows = groups * slot
     lanes = back_gate.shape[1]
@@ -452,8 +518,8 @@
     ffe = w_gate.shape[2]
     rows = groups * slot
     lanes = -(-slot // 128) * 128
-    stages = min(STAGES, groups)
-    span = rows // stages
+    stages = len(EIGHTHS) - 1
+    span = max(b - a for a, b in zip(EIGHTHS, EIGHTHS[1:])) * groups // 8 * slot
     vmem = pl.BlockSpec(memory_space=pltpu.VMEM)
     hbm = pl.BlockSpec(memory_space=pl.ANY)
     bf, f32 = jnp.bfloat16, jnp.float32
@@ -462,7 +528,7 @@
     twice = dma((2, groups))
     routes_t = routes.T
     weights_t = gate_weights.T
-    og, ou, od, back_rows, back_gate, places = pl.pallas_call(
+    og, ou, od, back_rows, back_gate, places, hidden, c_rows = pl.pallas_call(
         functools.partial(expert_kernel, groups, slot, quarter),
         out_shape=(
             pltpu.VMEM((width, ffe), bf),
@@ -471,17 +537,18 @@
             pltpu.VMEM((rows, quarter), bf),
             pltpu.VMEM((groups * SUM_ROWS, lanes), f32),
             pltpu.VMEM((8, tok_dev), jnp.int32),
+            pltpu.VMEM((rows, ffe), bf),
+            pltpu.VMEM((rows, width), bf),
         ),
         in_specs=[vmem, vmem, hbm, hbm, hbm, hbm, hbm],
-        out_specs=(vmem,) * 6,
+        out_specs=(vmem,) * 8,
         scratch_shapes=[
             pltpu.VMEM((tok_dev, width), bf),
             pltpu.VMEM((tok_dev, width), bf),
             pltpu.VMEM((rows, quarter), bf),
             pltpu.VMEM((rows, quarter), bf),
-            pltpu.VMEM((min(NEAR, groups) * slot, quarter), bf),
-            pltpu.VMEM((min(NEAR, groups) * slot, quarter), bf),
-            pltpu.VMEM((rows, width), bf),
+            pltpu.VMEM(((DIRECT[1] - DIRECT[0]) * slot, quarter), bf),
+            pltpu.VMEM(((DIRECT[1] - DIRECT[0]) * slot, quarter), bf),
             pltpu.VMEM((rows, width), bf),
             pltpu.VMEM((width, ffe), bf),
             pltpu.VMEM((width, ffe), bf),
@@ -492,13 +559,12 @@
             pltpu.VMEM((span, ffe), f32),
             pltpu.VMEM((span, ffe), f32),
             pltpu.VMEM((span, ffe), f32),
-            pltpu.VMEM((rows, ffe), bf),
             pltpu.VMEM((rows, 2 * ffe), bf),
             pltpu.VMEM((4, rows, quarter), bf),
             pltpu.VMEM((2, rows, quarter), bf),
             pltpu.VMEM((rows, quarter), bf),
             pltpu.VMEM((rows, quarter), bf),
-            pltpu.VMEM((4, groups * SUM_ROWS, lanes), f32),
+            pltpu.VMEM((4, groups, lanes), f32),
             pltpu.VMEM((groups * SUM_ROWS, lanes), f32),
             dma((5,)),
             twice, twice, twice, twice, twice, twice, twice, twice,
@@ -509,11 +575,11 @@
             dma((3,)),
         ],
         compiler_params=pltpu.CompilerParams(
-            collective_id=0, has_side_effects=True, vmem_limit_bytes=52 * 2 ** 20),
+            collective_id=0, has_side_effects=True, vmem_limit_bytes=46 * 2 ** 20),
         name="expert",
     )(routes_t, weights_t, tokens, cotangent, w_gate[0], w_up[0], w_down[0])
     held = [pltpu.with_memory_space_constraint(x, pltpu.VMEM)
-            for x in (places, back_rows, back_gate, og, ou, od)]
+            for x in (places, back_rows, back_gate, hidden, c_rows, og, ou, od)]
     grad_tokens, grad_gates, grad_gate_w, grad_up_w, grad_down = pl.pallas_call(
         functools.partial(collect_kernel, groups, slot),
         out_shape=(
@@ -523,10 +589,10 @@
             jax.ShapeDtypeStruct((width, ffe), bf),
             jax.ShapeDtypeStruct((ffe, width), bf),
         ),
-        in_specs=[vmem] * 7,
+        in_specs=[vmem] * 9,
         out_specs=(vmem, vmem, hbm, hbm, hbm),
-        scratch_shapes=[dma((3, 2))],
-        compiler_params=pltpu.CompilerParams(vmem_limit_bytes=8 * 2 ** 20),
+        scratch_shapes=[pltpu.VMEM((ffe, width), bf), dma((3, 4))],
+        compiler_params=pltpu.CompilerParams(vmem_limit_bytes=12 * 2 ** 20),
         name="collect",
     )(held[0], weights_t, *held[1:])
     return (grad_tokens, grad_gates.T, grad_gate_w[None], grad_up_w[None], grad_down[None])

time: 84.8 us -> 80.7 us (0.952)
  Pallas kernels: 83.8 us -> 79.4 us
    pallas_call x1, Pallas kernels: 78.8 us -> 74.5 us  [on_device(): pl.pallas_call(functools.partial(expert_kernel, groups, slot, quarter), o...]
where the time goes in v2:
time: 80.7 us; the launch traced here: 80.3 us
  Pallas kernels  79.4 us (98%)
  between operations  0.84 us (1%)
    pallas_call x1, Pallas kernels, on_device(): pl.pallas_call(functools.partial(expert_kernel, groups, slot, quarter), o...  74.5 us
    pallas_call x1, Pallas kernels, on_device(): pl.pallas_call(functools.partial(collect_kernel, groups, slot), out_shape...  4.93 us

profile of v2, /device:TPU:9, one launch (start us, length us, event | category | flops | bytes accessed | tf_op | source)
XLA Modules:
  0.0 80.3 jit_solution(137497183200017541)
XLA Ops:
  0.6 0.0 copy-start
  0.6 74.5 %expert.1 = (bf16[2048,896]{1,0:T(8,128)(2,1)S(1)}, bf16[2048,896]{1,0:T(8,128)(2,1)S(1)}, bf16[896,2048]{1,0:T(8,128)(2,1)S(1)}, bf16[768,512]{1,0:T(8,128)(2,1...) custom-call(s32[2,256]{1,0:T(2,128)} %bitcast.14, ...), custom_call_target="tpu_custom_call" | custom-call | tf_op jit(solution)/shard_map/expert/pallas_call | solution.py:531
  75.1 0.0 copy-done
  75.2 4.9 %collect.1 = (bf16[256,512]{1,0:T(8,128)(2,1)}, f32[2,256]{1,0:T(2,128)}, bf16[2048,896]{1,0:T(8,128)(2,1)}, bf16[2048,896]{1,0:T(8,128)(2,1)}, bf16[896,2048]{1,0:T(8,128)(2,1)}) custom-call(s32[8,256]{1,0:T(8,128)S(1)} %get-tuple-element.18.places, bf16[2,256]{1,0:T(2,128)(2,1)S(1)} %bitcast.10, bf16[768,512]{1,0:T(8,128)(2,1)S(1)} %get-tuple-element.19.back_rows, ...), custom_call_target="tpu_custom_call" | custom-call | tf_op jit(solution)/shard_map/collect/pallas_call | solution.py:583
Async XLA Ops:
  0.6 74.5 %copy-start = (bf16[256,2]{0,1:T(2,128)(2,1)S(1)}, bf16[256,2]{0,1:T(2,128)(2,1)}, u32[]{:S(2)}) copy-start(bf16[256,2]{0,1:T(2,128)(2,1)} %param.9) | copy-start | bytes 3076

commit v3 on v2

--- a/solution.py
+++ b/solution.py
@@ -292,9 +292,9 @@
         row_product(g, x_core_peer, 0)
         pair(g, 0).start()
         row_product(g, x_peer, 2)
-        crosses(g)
         row_product(g, core_peer, 1)
         pair(g, 1).start()
+        crosses(g)
         row_product(g, t, 3)
 
     def finish(g):

time: 80.7 us -> 80.7 us (level)
  no operation moved by 1% of the time
where the time goes in v3:
time: 80.7 us; the launch traced here: 80.3 us
  Pallas kernels  79.4 us (98%)
  between operations  0.84 us (1%)
    pallas_call x1, Pallas kernels, on_device(): pl.pallas_call(functools.partial(expert_kernel, groups, slot, quarter), o...  74.5 us
    pallas_call x1, Pallas kernels, on_device(): pl.pallas_call(functools.partial(collect_kernel, groups, slot), out_shape...  4.93 us

profile of v3, /device:TPU:9, one launch (start us, length us, event | category | flops | bytes accessed | tf_op | source)
XLA Modules:
  0.0 80.3 jit_solution(4029015537922049627)
XLA Ops:
  0.6 0.0 copy-start
  0.6 74.5 %expert.1 = (bf16[2048,896]{1,0:T(8,128)(2,1)S(1)}, bf16[2048,896]{1,0:T(8,128)(2,1)S(1)}, bf16[896,2048]{1,0:T(8,128)(2,1)S(1)}, bf16[768,512]{1,0:T(8,128)(2,1...) custom-call(s32[2,256]{1,0:T(2,128)} %bitcast.14, ...), custom_call_target="tpu_custom_call" | custom-call | tf_op jit(solution)/shard_map/expert/pallas_call | solution.py:531
  75.1 0.0 copy-done
  75.2 4.9 %collect.1 = (bf16[256,512]{1,0:T(8,128)(2,1)}, f32[2,256]{1,0:T(2,128)}, bf16[2048,896]{1,0:T(8,128)(2,1)}, bf16[2048,896]{1,0:T(8,128)(2,1)}, bf16[896,2048]{1,0:T(8,128)(2,1)}) custom-call(s32[8,256]{1,0:T(8,128)S(1)} %get-tuple-element.18.places, bf16[2,256]{1,0:T(2,128)(2,1)S(1)} %bitcast.10, bf16[768,512]{1,0:T(8,128)(2,1)S(1)} %get-tuple-element.19.back_rows, ...), custom_call_target="tpu_custom_call" | custom-call | tf_op jit(solution)/shard_map/collect/pallas_call | solution.py:583
Async XLA Ops:
  0.6 74.5 %copy-start = (bf16[256,2]{0,1:T(2,128)(2,1)S(1)}, bf16[256,2]{0,1:T(2,128)(2,1)}, u32[]{:S(2)}) copy-start(bf16[256,2]{0,1:T(2,128)(2,1)} %param.9) | copy-start | bytes 3076
